TPU v7x, 32 devices: a whole 2x2x4 slice. The times are simulated.
32 devices in a mesh: sp: 16 (over z, y, x), tp: 2 (over core).
Axes of the slice: x: 2, y: 2, z: 4, core: 2. Of those that a mesh axis runs over, the one named last changes fastest.
Arguments:
- query_logits: bfloat16 [2048, 1024], P('sp', 'tp'), may hold values from -6 to 6
- value_rows: bfloat16 [2048, 1024], P('sp', 'tp'), may hold values from -6 to 6
- onward_forget_logits: bfloat16 [2048, 1024], P('sp', 'tp'), may hold values from -5.5 to 5.5
- reverse_forget_logits: bfloat16 [2048, 1024], P('sp', 'tp'), may hold values from -5.5 to 5.5
- output_gate_logits: bfloat16 [2048, 1024], P('sp', 'tp'), may hold values from -6 to 6
- onward_floor_gap: float32 [1024], P('tp'), may hold values from 0 to 0.12, as said below
- reverse_floor_gap: float32 [1024], P('tp'), may hold values from 0 to 0.12, as said below
- extra_log_decay: float32 [2048, 8], P('sp', 'tp'), may hold values from -2.1 to 0
- per_head_gain: float32 [128], replicated, may hold values from 0.1 to 1.9
- residual: bfloat16 [2048, 2048], P('sp', 'tp'), may hold values from -8 to 8
- output_matrix: bfloat16 [1024, 2048], P(None, 'tp'), may hold values from -0.375 to 0.375
- inner_norm_gain: float32 [2048], P('tp'), may hold values from 0.1 to 1.9
- inner_norm_bias: float32 [2048], P('tp'), may hold values from -1.5 to 1.5
- gate_matrix: bfloat16 [2048, 5632], P('sp', 'tp'), may hold values from -0.125 to 0.125
- up_matrix: bfloat16 [2048, 5632], P('sp', 'tp'), may hold values from -0.125 to 0.125
- down_matrix: bfloat16 [5632, 2048], P('tp', 'sp'), may hold values from -0.15625 to 0.15625
- closing_norm_gain: float32 [2048], P('tp'), may hold values from 0.1 to 1.9
- closing_norm_bias: float32 [2048], P('tp'), may hold values from -1.5 to 1.5
Outputs:
- layer_output: bfloat16 [2048, 2048], P('sp', 'tp')
Inputs may be any that keep to these rules, and one draw needn't show every extreme that they name: `onward_floor_gap`: positive. `reverse_floor_gap`: positive.
All inputs are finite; a program needn't handle non-finite values.
Results may differ from a plain program's by a relative error of at most 0.014.
Values may be sent and summed in bfloat16 or wider, within the bound.
A program may use at most 128 MiB of HBM per device.

v0:
```python
import math
import jax
import jax.numpy as jnp
from jax import lax
from jax.sharding import PartitionSpec as P

D = 2048
highest_precision = lax.Precision.HIGHEST
alpha_mix = 2.0**0.25
norm_eps = 1e-05
head_eps = 1e-06


def prefix(x, axis, join, neutral, backward):
    count = lax.axis_size(axis)
    place = lax.axis_index(axis)
    ahead = count - 1 - place if backward else place
    gathered = jax.tree.map(
        lambda a, kind: lax.all_gather(a.astype(kind), axis), x, (jnp.bfloat16, jnp.bfloat16)
    )
    state = jax.tree.map(lambda a, e: jnp.zeros_like(a) + jnp.asarray(e, a.dtype), x, neutral)

    def one(step, state):
        source = count - 1 - step if backward else step
        return join(
            state,
            jax.tree.map(
                lambda a, own: lax.dynamic_index_in_dim(a, source, 0, False).astype(own.dtype),
                gathered,
                x,
            ),
        )

    return lax.fori_loop(0, ahead, one, state)


def decay_factors(unscaled_input, lower_bound_gap, extra_decays):
    decay_factor = lower_bound_gap * jax.nn.sigmoid(-unscaled_input.astype(jnp.float32))
    return (jnp.log1p(-decay_factor) + extra_decays, decay_factor)


def local_pass(query, keys, values, log_decay):
    rows, head_count, model_width = query.shape
    span = math.gcd(rows, 128)
    count = rows // span
    triangle = jnp.tril(jnp.ones((span, span), jnp.float32))

    def blocks(array):
        return array.reshape(count, span, head_count, array.shape[2])

    def advance(carry, inputs):
        running_state, offset = carry
        query_block, key_block, value_tile, log_block = inputs
        running = jnp.cumsum(log_block, axis=0)
        final_index = running[-1]
        decayed_query = query_block * jnp.exp(running)
        key_inverse = key_block * jnp.exp(-running)
        key_stop = key_block * jnp.exp(final_index[None] - running)
        scores = (
            jnp.einsum("thk,shk->hts", decayed_query, key_inverse, precision=highest_precision)
            * triangle[None]
        )
        inner = jnp.einsum("hts,shv->thv", scores, value_tile, precision=highest_precision)
        carried_state = jnp.einsum(
            "nex,exl->nel", decayed_query, running_state, precision=highest_precision
        )
        query_start = decayed_query * jnp.exp(offset)[None]
        running_state = jnp.exp(final_index)[:, :, None] * running_state + jnp.einsum(
            "ojy,oje->jye", key_stop, value_tile, precision=highest_precision
        )
        return ((running_state, offset + final_index), (inner + carried_state, query_start))

    start = (
        jnp.zeros((head_count, model_width, values.shape[2]), jnp.float32),
        jnp.zeros((head_count, model_width), jnp.float32),
    )
    final, outputs = lax.scan(
        advance, start, (blocks(query), blocks(keys), blocks(values), blocks(log_decay))
    )
    result = outputs[0].reshape(rows, head_count, values.shape[2])
    query_start = outputs[1].reshape(rows, head_count, model_width)
    return (result, query_start, final[1], final[0])


def join(earlier, later):
    return (earlier[0] + later[0], jnp.exp(later[0])[:, :, None] * earlier[1] + later[1])


def row_norm(before, moments, gain, bias):
    mean = moments[0] / D
    spread = moments[1] / D - mean * mean
    return (before - mean[:, None]) * lax.rsqrt(spread + norm_eps)[:, None] * gain + bias


def shards(
    query_logits,
    value_rows,
    onward_forget_logits,
    reverse_forget_logits,
    output_gate_logits,
    onward_floor_gap,
    reverse_floor_gap,
    extra_log_decay,
    per_head_gain,
    residual,
    output_matrix,
    inner_norm_gain,
    inner_norm_bias,
    gate_matrix,
    up_matrix,
    down_matrix,
    closing_norm_gain,
    closing_norm_bias,
):
    gate_whole, up_whole, down_whole = (
        lax.all_gather(gate_matrix, "sp", axis=0, tiled=True),
        lax.all_gather(up_matrix, "sp", axis=0, tiled=True),
        lax.all_gather(down_matrix, "sp", axis=1, tiled=True),
    )
    rows = query_logits.shape[0]
    head_count = extra_log_decay.shape[1]
    model_width = query_logits.shape[1] // head_count
    shape_head = (rows, head_count, model_width)
    query = jax.nn.silu(query_logits.astype(jnp.float32)).reshape(shape_head)
    values = value_rows.astype(jnp.float32).reshape(shape_head)
    extra_decays = jnp.repeat(extra_log_decay, model_width, axis=1)
    onward_log_decay, onward_key_rows = decay_factors(
        onward_forget_logits, onward_floor_gap, extra_decays
    )
    reverse_log_decay, reverse_key_rows = decay_factors(
        reverse_forget_logits, reverse_floor_gap, extra_decays
    )
    empty_total = jnp.zeros((head_count, model_width), jnp.float32)
    empty_state = jnp.zeros((head_count, model_width, model_width), jnp.float32)
    upcoming_part, upcoming_begin, ahead_total, ahead_state = local_pass(
        query, onward_key_rows.reshape(shape_head), values, onward_log_decay.reshape(shape_head)
    )
    incoming_state = prefix(
        (ahead_total, ahead_state), "sp", join, (empty_total, empty_state), False
    )
    upcoming_part = upcoming_part + jnp.einsum(
        "nex,exl->nel", upcoming_begin, incoming_state[1], precision=highest_precision
    )
    preceding_part, preceding_begin, behind_total, behind_state = local_pass(
        jnp.flip(query, axis=0),
        jnp.flip(reverse_key_rows.reshape(shape_head), axis=0),
        jnp.flip(values, axis=0),
        jnp.flip(reverse_log_decay.reshape(shape_head), axis=0),
    )
    arriving_state = prefix(
        (behind_total, behind_state), "sp", join, (empty_total, empty_state), True
    )
    preceding_part = jnp.flip(
        preceding_part
        + jnp.einsum(
            "nex,exl->nel", preceding_begin, arriving_state[1], precision=highest_precision
        ),
        axis=0,
    )
    mixed = upcoming_part + preceding_part
    normed = (
        mixed * lax.rsqrt(jnp.mean(mixed * mixed, axis=2, keepdims=True) + head_eps) * per_head_gain
    )
    gated = (
        normed.reshape(rows, head_count * model_width)
        * jax.nn.silu(output_gate_logits.astype(jnp.float32))
    ).astype(jnp.bfloat16)
    mixer = jnp.dot(
        lax.all_gather(gated, "tp", axis=1, tiled=True),
        output_matrix,
        preferred_element_type=jnp.float32,
    )
    before_middle = alpha_mix * residual.astype(jnp.float32) + mixer
    moments = lax.psum(
        (jnp.sum(before_middle, axis=1), jnp.sum(before_middle * before_middle, axis=1)), "tp"
    )
    middle = row_norm(before_middle, moments, inner_norm_gain, inner_norm_bias).astype(jnp.bfloat16)
    whole = lax.all_gather(middle, "tp", axis=1, tiled=True)
    gate = jnp.dot(whole, gate_whole, preferred_element_type=jnp.float32)
    up = jnp.dot(whole, up_whole, preferred_element_type=jnp.float32)
    hidden = (jax.nn.silu(gate) * up).astype(jnp.bfloat16)
    partial_value = jnp.dot(hidden, down_whole, preferred_element_type=jnp.float32)
    feed = lax.psum_scatter(
        partial_value.astype(jnp.bfloat16), "tp", scatter_dimension=1, tiled=True
    ).astype(jnp.float32)
    before_final = alpha_mix * middle.astype(jnp.float32) + feed
    closing = lax.psum(
        (jnp.sum(before_final, axis=1), jnp.sum(before_final * before_final, axis=1)), "tp"
    )
    return row_norm(before_final, closing, closing_norm_gain, closing_norm_bias).astype(
        jnp.bfloat16
    )


def solution(mesh):
    placed = (
        P("sp", "tp"),
        P("sp", "tp"),
        P("sp", "tp"),
        P("sp", "tp"),
        P("sp", "tp"),
        P("tp"),
        P("tp"),
        P("sp", "tp"),
        P(),
        P("sp", "tp"),
        P(None, "tp"),
        P("tp"),
        P("tp"),
        P("sp", "tp"),
        P("sp", "tp"),
        P("tp", "sp"),
        P("tp"),
        P("tp"),
    )
    return jax.shard_map(
        shards, mesh=mesh, in_specs=placed, out_specs=P("sp", "tp"), check_vma=False
    )
```

profile of v0, /device:TPU:0, one launch (start us, length us, event | category | flops | bytes accessed | tf_op | source)
XLA Modules:
  0.0 643.3 jit_solution(78488061301699797)
XLA Ops:
  6.5 0.9 copy.35
  7.7 2.1 bitcast_add_fusion.1
  10.3 1.7 reshape.106
  12.1 0.8 squeeze.50
  12.8 1.0 convert_multiply_fusion.1
  13.8 0.8 squeeze.48
  14.8 2.4 exponential_multiply_fusion.3
  17.2 1.3 fusion.7
  18.6 2.0 fusion.6
  22.6 44.0 %all_gather.38 = bf16[16,4,128]{2,1,0:T(4,128)(2,1)} all-gather(bf16[1,4,128]{2,1,0:T(4,128)(2,1)S(1)} %slice.20), channel_id=1, replica_groups=mesh['sp'=16,'tp'=2] {'sp'}, dimensions={0}, use_global_device_ids=true | all-gather | bytes 17408 | tf_op jit(solution)/shard_map/all_gather | solution.py:19
  66.7 35.8 %all_gather.35 = bf16[16,4,128]{2,1,0:T(4,128)(2,1)S(1)} all-gather(bf16[1,4,128]{2,1,0:T(4,128)(2,1)S(1)} %slice.21), channel_id=1, replica_groups=mesh['sp'=16,'tp'=2] {'sp'}, dimensions={0}, use_global_device_ids=true | all-gather | bytes 17408 | tf_op jit(solution)/shard_map/all_gather | solution.py:19
  102.5 1.6 convolution_multiply_fusion.2
  107.2 26.5 %while.17 = (s32[]{:T(128)}, f32[4,128,128]{2,1,0:T(8,128)S(1)}, s32[]{:T(128)}, bf16[16,4,128]{2,1,0:T(4,128)(2,1)}, bf16[16,4,128,128]{3,2,1,0:T(8,128)(2,1)},...) while((s32[]{:T(128)}, f32[4,128,128]{2,1,0:T(8,128)S(1)}, s32[]{:T(128)}, bf16[16,4,128]{2,1,0:T(4,128)(2,1)}, ...), condition=%wide.region_5.6_spmd, body=%wide.region_4.5_spmd.sunk | while | flops 197126 | bytes 660627 | solution.py:34
  107.8 1.1 convert_add_fusion.6
  109.6 1.1 convert_add_fusion.6
  110.7 0.7 exponential_bitcast_fusion.5
  111.4 1.1 convert_add_fusion.6
  113.1 1.1 convert_add_fusion.6
  114.8 1.1 convert_add_fusion.6
  116.6 1.1 convert_add_fusion.6
  118.3 1.1 convert_add_fusion.6
  119.4 0.7 exponential_bitcast_fusion.5
  120.1 1.1 convert_add_fusion.6
  121.9 1.1 convert_add_fusion.6
  123.0 0.7 exponential_bitcast_fusion.5
  123.7 1.1 convert_add_fusion.6
  125.5 1.1 convert_add_fusion.6
  127.2 1.1 convert_add_fusion.6
  129.0 1.1 convert_add_fusion.6
  130.1 0.7 exponential_bitcast_fusion.5
  130.8 1.1 convert_add_fusion.6
  132.5 1.1 convert_add_fusion.6
  133.6 1.3 fusion.1
  134.9 1.9 rev.20
  136.9 7.2 %all-gather.14.cloned.1.call-done = bf16[64,128,128]{2,1,0:T(8,128)(2,1)} async-done(((bf16[4,128,128]{2,1,0:T(8,128)(2,1)}), bf16[64,128,128]{2,1,0:T(8,128)(2,1)}) %all-gather.14.cloned.1.call-update) | async-done | bytes 2097168 | tf_op jit(solution)/shard_map/all_gather | solution.py:19
  144.7 0.7 multiply_multiply_fusion
  145.7 2.0 all_gather.41
  148.3 2.5 all-reduce.1
  151.0 2.4 all_gather.42
  153.3 133.7 %all-gather.8.cloned.1.call-done = bf16[2048,2816]{1,0:T(8,128)(2,1)} async-done(((bf16[128,2816]{1,0:T(8,128)(2,1)}), bf16[2048,2816]{1,0:T(8,128)(2,1)}) %all-gather.8.cloned.1.call-update) | async-done | bytes 11534352 | tf_op jit(solution)/shard_map/all_gather | solution.py:116
  287.0 7.0 %fusion.40 = f32[128,2816]{1,0:T(8,128)} fusion(bf16[128,2048]{1,0:T(8,128)(2,1)S(1)} %all_gather.42, bf16[2048,2816]{1,0:T(8,128)(2,1)} %all-gather.8.cloned.1.call-done), kind=kOutput, calls=%fused_computation.91 | convolution fusion | flops 1476395008 | bytes 13500416 | tf_op jit(solution)/shard_map/dot_general | solution.py:179
  294.1 135.2 %all-gather.10.cloned.1.call-done = bf16[2048,2816]{1,0:T(8,128)(2,1)} async-done(((bf16[128,2816]{1,0:T(8,128)(2,1)}), bf16[2048,2816]{1,0:T(8,128)(2,1)}) %all-gather.10.cloned.1.call-update) | async-done | bytes 11534352 | tf_op jit(solution)/shard_map/all_gather | solution.py:117
  429.3 182.8 %all-gather.12.cloned.1.call-done = bf16[2816,2048]{1,0:T(8,128)(2,1)} async-done(((bf16[2816,128]{1,0:T(8,128)(2,1)}), bf16[2816,2048]{1,0:T(8,128)(2,1)}) %all-gather.12.cloned.1.call-update) | async-done | bytes 11534352 | tf_op jit(solution)/shard_map/all_gather | solution.py:118
  612.1 12.3 %convolution_convert_fusion = bf16[128,2048]{1,0:T(8,128)(2,1)} fusion(bf16[2816,2048]{1,0:T(8,128)(2,1)} %all-gather.12.cloned.1.call-done, bf16[128,2048]{1,0:T(8,128)(2,1)S(1)} %all_gather.42, bf16[2048,2816]{1,0:T(8,128)(2,1)} %all-gather.10.cloned.1.call-done, f32[128,2816]{1,0:T(8,128)} %fusion.40), kind=kOutput, calls=%fused_computation.6 | convolution fusion | flops 2955214848 | bytes 25559040 | tf_op jit(solution)/shard_map/dot_general | solution.py:182
  624.4 6.3 reduce-scatter.2.cloned.1.call-done
  630.7 1.3 fusion.8
  632.0 2.5 all-reduce
  634.5 1.9 add_convert_fusion
  (74 shorter events, 14.7 us)
Async XLA Ops:
  6.5 141.2 %copy-start = (bf16[1024,1024]{1,0:T(8,128)(2,1)S(1)}, bf16[1024,1024]{1,0:T(8,128)(2,1)}, u32[]{:S(2)}) copy-start(bf16[1024,1024]{1,0:T(8,128)(2,1)} %param.32) | copy-start | bytes 6291460
  6.5 100.6 %all-gather.16.cloned.1.call-start = ((), (), s32[]{:S(2)}) async-start(), calls=%async_computation.6 | async-start | bytes 2228224 | tf_op jit(solution)/shard_map/all_gather | solution.py:19
  9.8 4.8 copy-start.1
  9.9 2.1 copy-start.2
  18.5 125.5 %all-gather.14.cloned.1.call-start = ((), (), s32[]{:S(2)}) async-start(), calls=%async_computation.5 | async-start | bytes 2228224 | tf_op jit(solution)/shard_map/all_gather | solution.py:19
  20.6 266.4 %all-gather.8.cloned.1.call-start = ((), (), s32[]{:S(2)}) async-start(), calls=%async_computation.1 | async-start | bytes 12255232 | tf_op jit(solution)/shard_map/all_gather | solution.py:116
  21.4 407.9 %all-gather.10.cloned.1.call-start = ((), (), s32[]{:S(2)}) async-start(), calls=%async_computation.2 | async-start | bytes 12255232 | tf_op jit(solution)/shard_map/all_gather | solution.py:117
  22.0 590.1 %all-gather.12.cloned.1.call-start = ((), (), s32[]{:S(2)}) async-start(), calls=%async_computation.3 | async-start | bytes 12255232 | tf_op jit(solution)/shard_map/all_gather | solution.py:118
  22.5 608.2 %reduce-scatter.2.cloned.1.call-start = ((), (), s32[]{:S(2)}) async-start(), calls=%async_computation.4 | async-start | bytes 786432 | tf_op jit(solution)/shard_map/reduce_scatter | solution.py:183
  22.6 82.6 %copy-start.3 = (f32[128,4,128]{2,1,0:T(4,128)S(1)}, f32[128,4,128]{2,1,0:T(4,128)}, u32[]{:S(2)}) copy-start(f32[128,4,128]{2,1,0:T(4,128)} %get-tuple-element.229) | copy-start | bytes 786436
  144.1 1.5 copy-start.5
  144.1 3.7 copy-start.4
  145.6 5.2 copy-start.6
  145.6 5.2 copy-start.7
  294.1 340.4 %copy-start.8 = (f32[1024]{0:T(1024)S(1)}, f32[1024]{0:T(1024)}, u32[]{:S(2)}) copy-start(f32[1024]{0:T(1024)} %param.39) | copy-start | bytes 12292
  294.1 340.4 %copy-start.9 = (f32[1024]{0:T(1024)S(1)}, f32[1024]{0:T(1024)}, u32[]{:S(2)}) copy-start(f32[1024]{0:T(1024)} %param.38) | copy-start | bytes 12292
Sparse Core Ops, SparseCore 0:
  18.7 63.2 all-gather.15
  84.7 59.2 all-gather.13
  146.8 140.2 all-gather.7
  289.7 139.5 all-gather.9
  431.8 180.2 all-gather.11
  624.5 6.1 reduce-scatter.1
where the time goes:
time: 644 us; the launch traced here: 643 us
  waiting for transfers between devices  467 us (73%)
  blocking collectives  89.1 us (14%)
  other arithmetic  36 us (6%)
  matrix products  29.8 us (5%)
  between operations  13.7 us (2%)
  local copies, waits for them, and re-layouts  6.96 us (1%)
    all_gather x1, waiting for transfers between devices, shards(): lax.all_gather(down_matrix, 'sp', axis=1, tiled=True)  183 us
    all_gather x1, waiting for transfers between devices, shards(): lax.all_gather(up_matrix, 'sp', axis=0, tiled=True)  135 us
    all_gather x1, waiting for transfers between devices, shards(): lax.all_gather(gate_matrix, 'sp', axis=0, tiled=True)  134 us
    all_gather x2, blocking collectives, prefix(): lax.all_gather(a.astype(kind), axis)  79.8 us
    add x15, other arithmetic, join(): jnp.exp(later[0])[:, :, None] * earlier[1] + later[1]  16.1 us
  transfers between devices with their start and end apart: 6, of which 5 were waited for; matrix products, arithmetic and copies ran while one was open for 7% of the time, Pallas kernels for 0%

commit v1 on v0

--- a/solution.py
+++ b/solution.py
@@ -112,10 +112,11 @@
     closing_norm_gain,
     closing_norm_bias,
 ):
+    recast_seats_all_on = lambda frame: jnp.concatenate(lax.all_gather(frame, "sp"), 1)
     gate_whole, up_whole, down_whole = (
         lax.all_gather(gate_matrix, "sp", axis=0, tiled=True),
         lax.all_gather(up_matrix, "sp", axis=0, tiled=True),
-        lax.all_gather(down_matrix, "sp", axis=1, tiled=True),
+        recast_seats_all_on(down_matrix),
     )
     rows = query_logits.shape[0]
     head_count = extra_log_decay.shape[1]

time: 644 us -> 605 us (0.939)
  waiting for transfers between devices: 467 us -> 421 us
  local copies, waits for them, and re-layouts: 6.96 us -> 22.1 us
  other arithmetic: 36 us -> 26.3 us
    all_gather x1, waiting for transfers between devices: 183 us -> 133 us  [shards(): lax.all_gather(frame, 'sp')]
    reshape x0 -> x1, local copies, waits for them, and re-layouts: none -> 15.2 us  [shards(): jnp.concatenate(lax.all_gather(frame, 'sp'), 1)]
    all_gather x2, waiting for transfers between devices: 7.19 us -> 17.9 us  [prefix(): lax.all_gather(a.astype(kind), axis)]
    exp x15, other arithmetic: 9.83 us -> 0.17 us  [join(): jnp.exp(later[0])[:, :, None] * earlier[1] + later[1]]
    all_gather x1, waiting for transfers between devices: 134 us -> 127 us  [shards(): lax.all_gather(gate_matrix, 'sp', axis=0, tiled=True)]
  transfers between devices with their start and end apart: 6 -> 6, of which waited for: 5 -> 5; matrix products, arithmetic and copies ran while one was open for 7% -> 9% of each run, Pallas kernels for 0% -> 0%
where the time goes in v1:
time: 605 us; the launch traced here: 604 us
  waiting for transfers between devices  421 us (70%)
  blocking collectives  87.8 us (15%)
  matrix products  32.2 us (5%)
  other arithmetic  26.3 us (4%)
  local copies, waits for them, and re-layouts  22.1 us (4%)
  between operations  13.7 us (2%)
    all_gather x1, waiting for transfers between devices, shards(): lax.all_gather(up_matrix, 'sp', axis=0, tiled=True)  135 us
    all_gather x1, waiting for transfers between devices, shards(): lax.all_gather(frame, 'sp')  133 us
    all_gather x1, waiting for transfers between devices, shards(): lax.all_gather(gate_matrix, 'sp', axis=0, tiled=True)  127 us
    all_gather x2, blocking collectives, prefix(): lax.all_gather(a.astype(kind), axis)  78.5 us
    all_gather x2, waiting for transfers between devices, prefix(): lax.all_gather(a.astype(kind), axis)  17.9 us
    add x15, other arithmetic, join(): jnp.exp(later[0])[:, :, None] * earlier[1] + later[1]  16.2 us
    reshape x1, local copies, waits for them, and re-layouts, shards(): jnp.concatenate(lax.all_gather(frame, 'sp'), 1)  15.2 us
    dot_general x1, matrix products, shards(): jnp.dot(hidden, down_whole, preferred_element_type=jnp.float32)  13.8 us
  transfers between devices with their start and end apart: 6, of which 5 were waited for; matrix products, arithmetic and copies ran while one was open for 9% of the time, Pallas kernels for 0%

profile of v1, /device:TPU:0, one launch (start us, length us, event | category | flops | bytes accessed | tf_op | source)
XLA Modules:
  0.0 604.0 jit_solution(4842596748376688466)
XLA Ops:
  6.5 0.9 copy.72
  7.7 2.0 bitcast_add_fusion.1
  10.2 1.7 reshape.112
  12.0 0.8 squeeze.50
  12.7 1.0 convert_multiply_fusion.1
  13.7 0.8 squeeze.48
  14.7 2.4 exponential_multiply_fusion.3
  17.1 1.3 fusion.7
  18.5 2.0 fusion.6
  20.6 0.7 all-gather.17.cloned.1.call-update
  22.5 42.6 %all_gather.41 = bf16[16,4,128]{2,1,0:T(4,128)(2,1)S(1)} all-gather(bf16[1,4,128]{2,1,0:T(4,128)(2,1)S(1)} %slice.20), channel_id=1, replica_groups=mesh['sp'=16,'tp'=2] {'sp'}, dimensions={0}, use_global_device_ids=true | all-gather | bytes 17408 | tf_op jit(solution)/shard_map/all_gather | solution.py:19
  65.1 35.8 %all_gather.38 = bf16[16,4,128]{2,1,0:T(4,128)(2,1)S(1)} all-gather(bf16[1,4,128]{2,1,0:T(4,128)(2,1)S(1)} %slice.21), channel_id=1, replica_groups=mesh['sp'=16,'tp'=2] {'sp'}, dimensions={0}, use_global_device_ids=true | all-gather | bytes 17408 | tf_op jit(solution)/shard_map/all_gather | solution.py:19
  101.0 1.6 convolution_multiply_fusion.2
  103.7 0.7 convolution_multiply_fusion.1
  105.7 17.0 %while.17 = (s32[]{:T(128)}, f32[4,128,128]{2,1,0:T(8,128)S(1)}, s32[]{:T(128)}, bf16[16,4,128]{2,1,0:T(4,128)(2,1)S(1)}, bf16[16,4,128,128]{3,2,1,0:T(8,128)(2,...) while((s32[]{:T(128)}, f32[4,128,128]{2,1,0:T(8,128)S(1)}, s32[]{:T(128)}, ...), condition=%wide.region_5.6_spmd, body=%wide.region_4.5_spmd.sunk | while | flops 197126 | bytes 660627 | solution.py:34
  105.7 1.1 convert_add_fusion.6
  106.9 1.1 convert_add_fusion.6
  108.0 1.1 convert_add_fusion.6
  109.2 1.1 convert_add_fusion.6
  110.3 1.1 convert_add_fusion.6
  111.4 1.1 convert_add_fusion.6
  112.5 1.1 convert_add_fusion.6
  113.7 1.1 convert_add_fusion.6
  114.8 1.1 convert_add_fusion.6
  115.9 1.1 convert_add_fusion.6
  117.0 1.1 convert_add_fusion.6
  118.2 1.1 convert_add_fusion.6
  119.3 1.1 convert_add_fusion.6
  120.4 1.1 convert_add_fusion.6
  121.6 1.1 convert_add_fusion.6
  122.7 1.3 fusion.1
  124.0 1.9 rev.20
  125.9 17.9 %all-gather.13.cloned.1.call-done = bf16[64,128,128]{2,1,0:T(8,128)(2,1)} async-done(((bf16[4,128,128]{2,1,0:T(8,128)(2,1)}), bf16[64,128,128]{2,1,0:T(8,128)(2,1)}) %all-gather.13.cloned.1.call-update) | async-done | bytes 2097168 | tf_op jit(solution)/shard_map/all_gather | solution.py:19
  144.5 0.7 multiply_multiply_fusion
  145.5 2.0 all_gather.44
  147.5 1.5 fusion.37
  149.0 2.5 all-reduce.1
  151.7 2.4 all_gather.45
  154.1 132.8 %all-gather.17.cloned.1.call-done = bf16[45056,128]{1,0:T(8,128)(2,1)} async-done(((bf16[2816,128]{1,0:T(8,128)(2,1)}), bf16[45056,128]{1,0:T(8,128)(2,1)}) %all-gather.17.cloned.1.call-update) | async-done | bytes 11534352 | tf_op jit(solution)/shard_map/all_gather | solution.py:115
  286.8 15.2 %copy.92 = bf16[2816,16,128]{0,2,1:T(8,128)(2,1)} copy(bf16[2816,16,128]{2,0,1:T(8,128)(2,1)} %bitcast.89) | data formatting | bytes 23068672 | tf_op jit(solution)/shard_map/reshape | solution.py:115
  302.0 127.1 %all-gather.9.cloned.1.call-done = bf16[2048,2816]{1,0:T(8,128)(2,1)} async-done(((bf16[128,2816]{1,0:T(8,128)(2,1)}), bf16[2048,2816]{1,0:T(8,128)(2,1)}) %all-gather.9.cloned.1.call-update) | async-done | bytes 11534352 | tf_op jit(solution)/shard_map/all_gather | solution.py:117
  429.1 7.1 %fusion.40 = f32[128,2816]{1,0:T(8,128)} fusion(bf16[128,2048]{1,0:T(8,128)(2,1)S(1)} %all_gather.45, bf16[2048,2816]{1,0:T(8,128)(2,1)} %all-gather.9.cloned.1.call-done), kind=kOutput, calls=%fused_computation.91 | convolution fusion | flops 1476395008 | bytes 13500416 | tf_op jit(solution)/shard_map/dot_general | solution.py:180
  436.2 135.2 %all-gather.11.cloned.1.call-done = bf16[2048,2816]{1,0:T(8,128)(2,1)} async-done(((bf16[128,2816]{1,0:T(8,128)(2,1)}), bf16[2048,2816]{1,0:T(8,128)(2,1)}) %all-gather.11.cloned.1.call-update) | async-done | bytes 11534352 | tf_op jit(solution)/shard_map/all_gather | solution.py:118
  571.3 13.8 %convolution_convert_fusion = bf16[128,2048]{1,0:T(8,128)(2,1)} fusion(bf16[2816,2048]{0,1:T(8,128)(2,1)} %bitcast.90, bf16[128,2048]{1,0:T(8,128)(2,1)S(1)} %all_gather.45, bf16[2048,2816]{1,0:T(8,128)(2,1)} %all-gather.11.cloned.1.call-done, f32[128,2816]{1,0:T(8,128)} %fusion.40), kind=kOutput, calls=%fused_computation.6 | convolution fusion | flops 2955214848 | bytes 25559040 | tf_op jit(solution)/shard_map/dot_general | solution.py:183
  585.2 6.3 %reduce-scatter.2.cloned.1.call-done = bf16[128,1024]{1,0:T(8,128)(2,1)} async-done(((bf16[128,2048]{1,0:T(8,128)(2,1)}), bf16[128,1024]{1,0:T(8,128)(2,1)}) %reduce-scatter.2.cloned.1.call-update) | async-done | bytes 262160 | tf_op jit(solution)/shard_map/reduce_scatter | solution.py:184
  591.4 1.3 fusion.8
  592.7 2.5 all-reduce
  595.2 1.9 add_convert_fusion
  (73 shorter events, 5.8 us)
Async XLA Ops:
  6.5 141.0 %copy-start = (bf16[1024,1024]{1,0:T(8,128)(2,1)S(1)}, bf16[1024,1024]{1,0:T(8,128)(2,1)}, u32[]{:S(2)}) copy-start(bf16[1024,1024]{1,0:T(8,128)(2,1)} %param.32) | copy-start | bytes 6291460
  6.5 99.1 %all-gather.15.cloned.1.call-start = ((), (), s32[]{:S(2)}) async-start(), calls=%async_computation.5 | async-start | bytes 2228224 | tf_op jit(solution)/shard_map/all_gather | solution.py:19
  9.8 4.8 copy-start.2
  18.4 125.4 %all-gather.13.cloned.1.call-start = ((), (), s32[]{:S(2)}) async-start(), calls=%async_computation.4 | async-start | bytes 2228224 | tf_op jit(solution)/shard_map/all_gather | solution.py:19
  20.5 266.3 %all-gather.17.cloned.1.call-start = ((), (), s32[]{:S(2)}) async-start(), calls=%async_computation.6 | async-start | bytes 12255232 | tf_op jit(solution)/shard_map/all_gather | solution.py:115
  21.3 407.8 %all-gather.9.cloned.1.call-start = ((), (), s32[]{:S(2)}) async-start(), calls=%async_computation.1 | async-start | bytes 12255232 | tf_op jit(solution)/shard_map/all_gather | solution.py:117
  21.8 549.5 %all-gather.11.cloned.1.call-start = ((), (), s32[]{:S(2)}) async-start(), calls=%async_computation.2 | async-start | bytes 12255232 | tf_op jit(solution)/shard_map/all_gather | solution.py:118
  22.4 569.0 %reduce-scatter.2.cloned.1.call-start = ((), (), s32[]{:S(2)}) async-start(), calls=%async_computation.3 | async-start | bytes 786432 | tf_op jit(solution)/shard_map/reduce_scatter | solution.py:184
  22.5 81.2 %copy-start.3 = (f32[128,4,128]{2,1,0:T(4,128)S(1)}, f32[128,4,128]{2,1,0:T(4,128)}, u32[]{:S(2)}) copy-start(f32[128,4,128]{2,1,0:T(4,128)} %get-tuple-element.229) | copy-start | bytes 786436
  143.8 1.6 copy-start.4
  145.4 6.1 %copy-start.5 = (f32[1024]{0:T(1024)S(1)}, f32[1024]{0:T(1024)}, u32[]{:S(2)}) copy-start(f32[1024]{0:T(1024)} %param.34) | copy-start | bytes 12292
  145.4 6.1 %copy-start.6 = (f32[1024]{0:T(1024)S(1)}, f32[1024]{0:T(1024)}, u32[]{:S(2)}) copy-start(f32[1024]{0:T(1024)} %param.33) | copy-start | bytes 12292
  571.3 23.8 %copy-start.7 = (f32[1024]{0:T(1024)S(1)}, f32[1024]{0:T(1024)}, u32[]{:S(2)}) copy-start(f32[1024]{0:T(1024)} %param.39) | copy-start | bytes 12292
  571.3 23.8 %copy-start.8 = (f32[1024]{0:T(1024)S(1)}, f32[1024]{0:T(1024)}, u32[]{:S(2)}) copy-start(f32[1024]{0:T(1024)} %param.38) | copy-start | bytes 12292
  571.3 25.8 %copy-start.1 = (bf16[1024,1024]{1,0:T(8,128)(2,1)S(1)}, bf16[1024,1024]{1,0:T(8,128)(2,1)}, u32[]{:S(2)}) copy-start(bf16[1024,1024]{1,0:T(8,128)(2,1)} %param.32) | copy-start | bytes 6291460
Sparse Core Ops, SparseCore 0:
  18.5 63.2 all-gather.14
  84.6 59.1 all-gather.12
  146.6 140.2 all-gather.16
  289.5 139.5 all-gather.8
  431.7 139.5 all-gather.10
  585.3 6.0 reduce-scatter.1
